TPU v7x, 32 devices: a whole 2x2x4 slice. The times are simulated.
32 devices in a mesh: sp: 8 (over z, x), tp: 4 (over y, core).
Axes of the slice: x: 2, y: 2, z: 4, core: 2. Of those that a mesh axis runs over, the one named last changes fastest.
Arguments:
- tokens: bfloat16 [3072, 2048], P('sp', 'tp'), may hold values from -6 to 6
- norm_gain: float32 [2048], replicated, may hold values from 0.1 to 1.9
- w_pool_in: bfloat16 [2048, 2048], P('sp', 'tp'), may hold values from -0.125 to 0.125
- w_lru_in: bfloat16 [2048, 2048], P('sp', 'tp'), may hold values from -0.125 to 0.125
- pool_mix: bfloat16 [4, 512, 512], P('tp'), may hold values from -0.25 to 0.25
- conv_taps: bfloat16 [4, 2048], P(None, 'tp'), may hold values from -3 to 3
- rec_gate: bfloat16 [2, 16, 128, 128], P(None, 'tp'), may hold values from -0.5 to 0.5
- in_gate: bfloat16 [2, 16, 128, 128], P(None, 'tp'), may hold values from -0.5 to 0.5
- decay_rate: float32 [2, 2048], P(None, 'tp'), may hold values from 0 to 1, as said below
- log_decay: float32 [2, 3072], P(None, 'sp'), may hold values from -2 to 0, as said below
- start_state: float32 [2, 2048], P(None, 'tp'), may hold values from -8 to 8
- w_out_pool: bfloat16 [2048, 2048], P('tp', 'sp'), may hold values from -0.09375 to 0.09375
- w_out_lru: bfloat16 [2048, 2048], P('tp', 'sp'), may hold values from -0.09375 to 0.09375
Outputs:
- mixed: bfloat16 [3072, 2048], P(('sp', 'tp'))
Inputs may be any that keep to these rules, and one draw needn't show every extreme that they name: `decay_rate`: positive. `log_decay`: at most zero.
All inputs are finite; a program needn't handle non-finite values.
Results may differ from a plain program's by a relative error of at most 0.0068.
Values may be sent and summed in bfloat16 or wider, within the bound.
A program may use at most 64 MiB of HBM per device.

v0:
```python
import jax
import jax.numpy as jnp
from jax import lax
from jax.sharding import PartitionSpec as P

POOL_GROUPS = 4
GRID_W = 32


epsilon = 1e-06


def with_halo(cells, sides, width):
    for axis, dim in sides:
        count = lax.axis_size(axis)
        ends = count - 1
        head = lax.slice_in_dim(cells, 0, width, axis=dim)
        tail = lax.slice_in_dim(cells, cells.shape[dim] - width, cells.shape[dim], axis=dim)
        cells = jnp.concatenate(
            [
                lax.ppermute(tail, axis, [(i, (i + 1) % count) for i in range(ends)]),
                cells,
                lax.ppermute(head, axis, [((i + 1) % count, i) for i in range(ends)]),
            ],
            axis=dim,
        )
    return cells


def link_pair(earlier, later_pair):
    return (earlier[0] * later_pair[0], later_pair[0] * earlier[1] + later_pair[1])


def per_device(
    tokens,
    norm_gain,
    w_pool_in,
    w_lru_in,
    pool_mix,
    conv_taps,
    rec_gate,
    in_gate,
    decay_rate,
    log_decay,
    start_state,
    w_out_pool,
    w_out_lru,
):
    tok_rows = tokens.shape[0]
    pool_width = w_pool_in.shape[1]
    lru_width = w_lru_in.shape[1]
    whole_rows = lax.all_gather(tokens, "tp", axis=1, tiled=True)
    values = whole_rows.astype(jnp.float32)
    root_mean_square_scale = lax.rsqrt(jnp.mean(values * values, axis=1, keepdims=True) + epsilon)
    normed = (values * root_mean_square_scale * norm_gain).astype(jnp.bfloat16)
    sum_pool = jnp.dot(
        normed,
        lax.all_gather(w_pool_in, "sp", axis=0, tiled=True),
        preferred_element_type=jnp.float32,
    )
    sum_lru = jnp.dot(
        normed,
        lax.all_gather(w_lru_in, "sp", axis=0, tiled=True),
        preferred_element_type=jnp.float32,
    )
    u_pool = sum_pool.astype(jnp.bfloat16)
    u_lru = sum_lru.astype(jnp.bfloat16)
    grid_rows = tok_rows // GRID_W
    reach = 2 ** (POOL_GROUPS - 1)
    grid_pooled_image = u_pool.reshape(grid_rows, GRID_W, pool_width)
    extended = with_halo(grid_pooled_image, (("sp", 0),), reach)
    half_span = jnp.left_shift(jnp.int32(1), lax.axis_index("tp"))
    row_count = grid_rows * lax.axis_size("sp")
    first_row = lax.axis_index("sp") * grid_rows
    local_rows = first_row + jnp.arange(grid_rows, dtype=jnp.int32)
    row_lower = jnp.clip(local_rows - half_span, 0, row_count)
    row_upper = jnp.clip(local_rows + half_span, 0, row_count)
    halo_rows = first_row - reach + jnp.arange(grid_rows + 2 * reach, dtype=jnp.int32)
    row_box = (
        (halo_rows[None, :] >= row_lower[:, None]) & (halo_rows[None, :] < row_upper[:, None])
    ).astype(jnp.bfloat16)
    col_index = jnp.arange(GRID_W, dtype=jnp.int32)
    col_lower = jnp.clip(col_index - half_span, 0, GRID_W)
    col_upper = jnp.clip(col_index + half_span, 0, GRID_W)
    col_box = (
        (col_index[None, :] >= col_lower[:, None]) & (col_index[None, :] < col_upper[:, None])
    ).astype(jnp.float32)
    row_sums = jnp.einsum("ae,ecz->acz", row_box, extended, preferred_element_type=jnp.float32)
    box_total = jnp.einsum("bc,acz->abz", col_box, row_sums, precision=lax.Precision.HIGHEST)
    counts = ((row_upper - row_lower)[:, None] * (col_upper - col_lower)[None, :]).astype(
        jnp.float32
    )
    pool_diff = (box_total / counts[:, :, None] - grid_pooled_image.astype(jnp.float32)).astype(
        jnp.bfloat16
    )
    y_pool = jnp.dot(
        pool_diff.reshape(tok_rows, pool_width), pool_mix[0], preferred_element_type=jnp.float32
    ).astype(jnp.bfloat16)
    tap_count = conv_taps.shape[0]
    left_taps = tap_count // 2
    padded = with_halo(u_lru, (("sp", 0),), left_taps)
    tap_weights = conv_taps.astype(jnp.float32)
    conv_sum = padded[0:tok_rows].astype(jnp.float32) * tap_weights[0]
    for tap_index in range(1, tap_count):
        conv_sum = (
            conv_sum
            + padded[tap_index : tap_index + tok_rows].astype(jnp.float32) * tap_weights[tap_index]
        )
    conv_in = conv_sum.astype(jnp.bfloat16)
    head_size = rec_gate.shape[2]
    blocks = conv_in.reshape(tok_rows, lru_width // head_size, head_size)
    drive_in = conv_in.astype(jnp.float32)
    local_scans = []
    for direction in range(2):
        recur_gate = jax.nn.sigmoid(
            jnp.einsum(
                "tnc,ncd->tnd", blocks, rec_gate[direction], preferred_element_type=jnp.float32
            ).reshape(tok_rows, lru_width)
        )
        input_gate = jax.nn.sigmoid(
            jnp.einsum(
                "tnc,ncd->tnd", blocks, in_gate[direction], preferred_element_type=jnp.float32
            ).reshape(tok_rows, lru_width)
        )
        log_keep = -8.0 * recur_gate * decay_rate[direction] + log_decay[direction][:, None]
        keep_rate = jnp.exp(log_keep)
        drive_term = jnp.sqrt(-jnp.expm1(2.0 * log_keep)) * input_gate * drive_in
        local_scans.append(
            lax.associative_scan(link_pair, (keep_rate, drive_term), reverse=direction == 1, axis=0)
        )
    forward_prod, leftward_running_total = local_scans[0]
    reverse_decay_product, backward_sum = local_scans[1]
    unit_rate = jnp.ones((lru_width,), jnp.float32)
    nothing = jnp.zeros((lru_width,), jnp.float32)
    summary_prod = jnp.stack([forward_prod[-1], reverse_decay_product[0]])[None]
    summary_sum = jnp.stack([leftward_running_total[-1], backward_sum[0]])[None]
    every_prod, every_sum = (
        lax.all_gather(summary_prod, "sp", axis=0, tiled=True),
        lax.all_gather(summary_sum, "sp", axis=0, tiled=True),
    )
    sequence_index = lax.axis_index("sp")
    unit_row = unit_rate[None]
    nothing_row = nothing[None]
    run_forward = lax.associative_scan(link_pair, (every_prod[:, 0], every_sum[:, 0]), axis=0)
    run_backward = lax.associative_scan(
        link_pair, (every_prod[:, 1], every_sum[:, 1]), reverse=True, axis=0
    )
    enter_forward = (
        lax.dynamic_index_in_dim(
            jnp.concatenate([unit_row, run_forward[0]], axis=0), sequence_index, 0, keepdims=False
        ),
        lax.dynamic_index_in_dim(
            jnp.concatenate([nothing_row, run_forward[1]], axis=0),
            sequence_index,
            0,
            keepdims=False,
        ),
    )
    enter_backward = (
        lax.dynamic_index_in_dim(
            jnp.concatenate([run_backward[0], unit_row], axis=0),
            sequence_index + 1,
            0,
            keepdims=False,
        ),
        lax.dynamic_index_in_dim(
            jnp.concatenate([run_backward[1], nothing_row], axis=0),
            sequence_index + 1,
            0,
            keepdims=False,
        ),
    )
    state_forward = enter_forward[0] * start_state[0] + enter_forward[1]
    state_backward = enter_backward[0] * start_state[1] + enter_backward[1]
    y_lru = (
        forward_prod * state_forward
        + leftward_running_total
        + reverse_decay_product * state_backward
        + backward_sum
    ).astype(jnp.bfloat16)
    weight_pool, weight_lru = (
        lax.all_gather(w_out_pool, "sp", axis=1, tiled=True),
        lax.all_gather(w_out_lru, "sp", axis=1, tiled=True),
    )
    mixed = lax.psum_scatter(
        jnp.dot(y_pool, weight_pool, preferred_element_type=jnp.float32)
        + jnp.dot(y_lru, weight_lru, preferred_element_type=jnp.float32),
        "tp",
        scatter_dimension=0,
        tiled=True,
    )
    return mixed.astype(jnp.bfloat16)


def solution(mesh):
    placed = (
        P("sp", "tp"),
        P(),
        P("sp", "tp"),
        P("sp", "tp"),
        P("tp", None, None),
        P(None, "tp"),
        P(None, "tp", None, None),
        P(None, "tp", None, None),
        P(None, "tp"),
        P(None, "sp"),
        P(None, "tp"),
        P("tp", "sp"),
        P("tp", "sp"),
    )
    return jax.shard_map(
        per_device, mesh=mesh, in_specs=placed, out_specs=P(("sp", "tp"), None), check_vma=False
    )
```

profile of v0, /device:TPU:3, one launch (start us, length us, event | category | flops | bytes accessed | tf_op | source)
XLA Modules:
  0.0 541.0 jit_solution(16455500868472331515)
XLA Ops:
  14.7 15.5 %all-gather.10.cloned.1.call-done = bf16[384,2048]{1,0:T(8,128)(2,1)} async-done(((bf16[384,512]{1,0:T(8,128)(2,1)}), bf16[384,2048]{1,0:T(8,128)(2,1)}) %all-gather.10.cloned.1.call-update) | async-done | bytes 1572880 | tf_op jit(solution)/shard_map/all_gather | solution.py:52
  30.2 1.8 fusion
  32.0 46.2 %all-gather.16.cloned.1.call-done = bf16[2048,512]{1,0:T(8,128)(2,1)} async-done(((bf16[256,512]{1,0:T(8,128)(2,1)}), bf16[2048,512]{1,0:T(8,128)(2,1)}) %all-gather.16.cloned.1.call-update) | async-done | bytes 2097168 | tf_op jit(solution)/shard_map/all_gather | solution.py:63
  78.2 3.1 convolution_convert_fusion
  81.3 4.9 collective-permute-start.2
  86.2 2.1 collective-permute-start.3
  88.3 39.7 %all-gather.12.cloned.1.call-done = bf16[2048,512]{1,0:T(8,128)(2,1)} async-done(((bf16[256,512]{1,0:T(8,128)(2,1)}), bf16[2048,512]{1,0:T(8,128)(2,1)}) %all-gather.12.cloned.1.call-update) | async-done | bytes 2097168 | tf_op jit(solution)/shard_map/all_gather | solution.py:58
  128.0 3.1 convolution_convert_fusion.2
  132.1 4.9 collective-permute-start
  137.0 1.9 collective-permute-start.1
  142.4 2.3 copy.43
  148.1 3.7 fusion.22
  154.7 3.2 slice.903
  157.8 3.2 slice.904
  161.0 2.2 fusion.97
  164.7 1.7 slice.906
  166.4 1.7 slice.907
  168.0 2.0 fusion.101
  171.3 1.6 slice.909
  172.9 1.6 slice.910
  174.5 1.7 fusion.103
  219.1 1.6 slice.935
  223.4 1.7 slice.937
  228.5 3.2 slice.939
  237.7 4.5 slice.846
  242.2 4.5 slice.848
  246.8 4.5 slice.944
  251.3 2.7 slice.946
  254.0 2.3 fusion.98
  257.7 1.7 slice.948
  259.4 1.7 slice.949
  261.1 1.9 fusion.102
  264.3 1.6 slice.951
  265.9 1.6 slice.952
  267.5 1.7 fusion.104
  310.8 1.6 slice.977
  315.1 1.7 slice.979
  333.6 2.0 pad.329
  337.4 2.2 add_multiply_fusion.3
  339.7 1.9 pad.328
  358.1 2.3 pad.302
  361.0 1.6 add.631
  362.7 1.9 add_multiply_fusion.6
  366.3 2.5 pad.343
  368.8 1.8 add.687
  370.6 2.8 pad.345
  375.1 2.5 pad.305
  377.6 4.7 slice.884
  382.3 4.7 slice.982
  387.0 2.5 add_multiply_fusion.2
  390.2 2.9 pad.344
  394.6 23.3 %all-gather.3 = f32[8,2,512]{2,1,0:T(2,128)S(1)} all-gather(f32[1,2,512]{2,1,0:T(2,128)S(1)} %maximum_bitcast_fusion.1), channel_id=3, replica_groups=mesh['sp'=8,'tp'=4] {'sp'}, dimensions={0}, use_global_device_ids=true | all-gather | bytes 36864 | tf_op jit(solution)/shard_map/all_gather | solution.py:139
  418.8 1.9 add.632
  422.1 2.9 pad.307
  425.0 1.9 pad.306
  427.8 24.2 %all-gather.2 = f32[8,2,512]{2,1,0:T(2,128)S(1)} all-gather(f32[1,2,512]{2,1,0:T(2,128)S(1)} %maximum_bitcast_fusion), channel_id=2, replica_groups=mesh['sp'=8,'tp'=4] {'sp'}, dimensions={0}, use_global_device_ids=true | all-gather | bytes 36864 | tf_op jit(solution)/shard_map/all_gather | solution.py:138
  454.1 1.5 add.633
  457.1 4.0 rev.16
  461.1 4.0 rev.19
  467.1 1.8 fusion.17
  468.9 4.7 fusion.18
  473.6 6.0 %convolution_add_fusion = f32[384,2048]{1,0:T(8,128)} fusion(f32[384,2048]{1,0:T(8,128)} %fusion.18, bf16[512,2048]{1,0:T(8,128)(2,1)} %all-gather.18.cloned.1.call-done, f32[384,512]{1,0:T(8,128)} %rev.19, f32[384,512]{1,0:T(8,128)} %rev.16, f32[384,512]{1,0:T(8,128)S(1)} %copy-done.4, f32[384,512]{1,0:T(8,128)S(1)} %copy-done.3, f32[384,512]{1,0:T(8,128)} %copy-done.5, ...), kind=kOutput, calls=%fused_computation.5 | convolution fusion | flops 807665664 | bytes 13111296 | tf_op jit(solution)/shard_map/dot_general | solution.py:187
  479.7 52.6 %reduce-scatter.2.cloned.1.call-done = f32[96,2048]{1,0:T(8,128)} async-done(((f32[384,2048]{1,0:T(8,128)}), f32[96,2048]{1,0:T(8,128)}) %reduce-scatter.2.cloned.1.call-update) | async-done | bytes 786448 | tf_op jit(solution)/shard_map/reduce_scatter | solution.py:185
  532.2 1.9 convert_element_type.73
  (443 shorter events, 172.8 us)
Async XLA Ops:
  6.5 462.4 %copy-start = (bf16[1,512,512]{2,1,0:T(8,128)(2,1)S(1)}, bf16[1,512,512]{2,1,0:T(8,128)(2,1)}, u32[]{:S(2)}) copy-start(bf16[1,512,512]{2,1,0:T(8,128)(2,1)} %param.17) | copy-start | bytes 1572868
  6.5 71.7 %copy-start.41 = (f32[2048]{0:T(1024)S(1)}, f32[2048]{0:T(1024)}, u32[]{:S(2)}) copy-start(f32[2048]{0:T(1024)} %param.14) | copy-start | bytes 24580
  6.5 23.6 %all-gather.10.cloned.1.call-start = ((), (), s32[]{:S(2)}) async-start(), calls=%async_computation.1 | async-start | bytes 1966080 | tf_op jit(solution)/shard_map/all_gather | solution.py:52
  7.3 70.9 %all-gather.16.cloned.1.call-start = ((), (), s32[]{:S(2)}) async-start(), calls=%async_computation.4 | async-start | bytes 2359296 | tf_op jit(solution)/shard_map/all_gather | solution.py:63
  8.0 120.0 %all-gather.12.cloned.1.call-start = ((), (), s32[]{:S(2)}) async-start(), calls=%async_computation.2 | async-start | bytes 2359296 | tf_op jit(solution)/shard_map/all_gather | solution.py:58
  8.7 460.2 %all-gather.14.cloned.1.call-start = ((), (), s32[]{:S(2)}) async-start(), calls=%async_computation.3 | async-start | bytes 2359296 | tf_op jit(solution)/shard_map/all_gather | solution.py:182
  9.3 464.3 %all-gather.18.cloned.1.call-start = ((), (), s32[]{:S(2)}) async-start(), calls=%async_computation.5 | async-start | bytes 2359296 | tf_op jit(solution)/shard_map/all_gather | solution.py:183
  9.9 522.3 %reduce-scatter.2.cloned.1.call-start = ((), (), s32[]{:S(2)}) async-start(), calls=%async_computation.6 | async-start | bytes 3932160 | tf_op jit(solution)/shard_map/reduce_scatter | solution.py:185
  81.3 57.6 %collective-permute-start.2 = (bf16[2,512]{1,0:T(2,128)(2,1)S(1)}, bf16[2,512]{1,0:T(2,128)(2,1)S(1)}, u32[]{:S(2)}, u32[]{:S(2)}) collective-permute-start(bf16[2,512]{1,0:T(2,128)(2,1)S(1)} %get-tuple-element.31), channel_id=1, source_target_pairs={{0,4},{4,8},{8,12},{12,16},{16,20},{20,24},{24,28},{1,5},{5,9},{9,... | collective-permute-start | bytes 6152 | tf_op jit(solution)/shard_map/ppermute | solution.py:21
  86.2 53.1 %copy-start.39 = (bf16[2,4,128,128]{3,2,1,0:T(8,128)(2,1)S(1)}, bf16[2,4,128,128]{3,2,1,0:T(8,128)(2,1)}, u32[]{:S(2)}) copy-start(bf16[2,4,128,128]{3,2,1,0:T(8,128)(2,1)} %param.19) | copy-start | bytes 786436
  86.2 52.7 %collective-permute-start.3 = (bf16[2,512]{1,0:T(2,128)(2,1)S(1)}, bf16[2,512]{1,0:T(2,128)(2,1)S(1)}, u32[]{:S(2)}, u32[]{:S(2)}) collective-permute-start(bf16[2,512]{1,0:T(2,128)(2,1)S(1)} %get-tuple-element.30), channel_id=1, source_target_pairs={{4,0},{8,4},{12,8},{16,12},{20,16},{24,20},{28,24},{5,1},{9,5},{13... | collective-permute-start | bytes 6152 | tf_op jit(solution)/shard_map/ppermute | solution.py:23
  131.1 9.5 %copy-start.9 = (bf16[384,512]{1,0:T(8,128)(2,1)}, bf16[384,512]{1,0:T(8,128)(2,1)S(1)}, u32[]{:S(2)}) copy-start(bf16[384,512]{1,0:T(8,128)(2,1)S(1)} %convolution_convert_fusion.2) | copy-start | bytes 1179652
  132.1 333.1 %collective-permute-start = (bf16[8,32,512]{2,1,0:T(8,128)(2,1)}, bf16[8,32,512]{2,1,0:T(8,128)(2,1)}, u32[]{:S(2)}, u32[]{:S(2)}) collective-permute-start(bf16[8,32,512]{2,1,0:T(8,128)(2,1)} %bitcast.1), channel_id=1, source_target_pairs={{0,4},{4,8},{8,12},{12,16},{16,20},{20,24},{24,28},{1,5},{5,9},{9,... | collective-permute-start | bytes 786440 | tf_op jit(solution)/shard_map/ppermute | solution.py:21
  137.0 328.2 %collective-permute-start.1 = (bf16[8,32,512]{2,1,0:T(8,128)(2,1)}, bf16[8,32,512]{2,1,0:T(8,128)(2,1)}, u32[]{:S(2)}, u32[]{:S(2)}) collective-permute-start(bf16[8,32,512]{2,1,0:T(8,128)(2,1)} %bitcast.3), channel_id=1, source_target_pairs={{4,0},{8,4},{12,8},{16,12},{20,16},{24,20},{28,24},{5,1},{9,5},{13... | collective-permute-start | bytes 786440 | tf_op jit(solution)/shard_map/ppermute | solution.py:23
  140.6 1.0 copy-start.40
  318.6 7.3 %copy-start.33 = (f32[1,512]{1,0:T(1,128)S(1)}, f32[1,512]{1,0:T(1,128)}, u32[]{:S(2)}) copy-start(f32[1,512]{1,0:T(1,128)} %slice.1110) | copy-start | bytes 6148
  318.6 7.3 %copy-start.32 = (f32[1,512]{1,0:T(1,128)S(1)}, f32[1,512]{1,0:T(1,128)}, u32[]{:S(2)}) copy-start(f32[1,512]{1,0:T(1,128)} %slice.1048) | copy-start | bytes 6148
  318.6 7.4 %copy-start.20 = (f32[11,512]{1,0:T(8,128)S(1)}, f32[11,512]{1,0:T(8,128)}, u32[]{:S(2)}) copy-start(f32[11,512]{1,0:T(8,128)} %slice.831) | copy-start | bytes 67588
  318.6 7.4 %copy-start.21 = (f32[11,512]{1,0:T(8,128)S(1)}, f32[11,512]{1,0:T(8,128)}, u32[]{:S(2)}) copy-start(f32[11,512]{1,0:T(8,128)} %slice.931) | copy-start | bytes 67588
  318.6 7.5 %copy-start.31 = (f32[1,512]{1,0:T(1,128)S(1)}, f32[1,512]{1,0:T(1,128)}, u32[]{:S(2)}) copy-start(f32[1,512]{1,0:T(1,128)} %slice.1109) | copy-start | bytes 6148
  318.6 7.5 %copy-start.30 = (f32[1,512]{1,0:T(1,128)S(1)}, f32[1,512]{1,0:T(1,128)}, u32[]{:S(2)}) copy-start(f32[1,512]{1,0:T(1,128)} %slice.1047) | copy-start | bytes 6148
  318.6 9.2 %copy-start.29 = (f32[1,512]{1,0:T(1,128)S(1)}, f32[1,512]{1,0:T(1,128)}, u32[]{:S(2)}) copy-start(f32[1,512]{1,0:T(1,128)} %slice.1046) | copy-start | bytes 6148
  321.5 7.0 %copy-start.18 = (f32[47,512]{1,0:T(8,128)S(1)}, f32[47,512]{1,0:T(8,128)}, u32[]{:S(2)}) copy-start(f32[47,512]{1,0:T(8,128)} %slice.835) | copy-start | bytes 288772
  321.5 7.0 %copy-start.19 = (f32[47,512]{1,0:T(8,128)S(1)}, f32[47,512]{1,0:T(8,128)}, u32[]{:S(2)}) copy-start(f32[47,512]{1,0:T(8,128)} %slice.935) | copy-start | bytes 288772
  325.1 3.5 copy-start.27
  327.9 3.9 copy-start.13
  327.9 3.9 copy-start.14
  333.6 2.1 copy-start.2
  336.4 3.3 copy-start.26
  341.6 9.5 %copy-start.28 = (f32[1,512]{1,0:T(1,128)S(1)}, f32[1,512]{1,0:T(1,128)}, u32[]{:S(2)}) copy-start(f32[1,512]{1,0:T(1,128)} %slice.1072) | copy-start | bytes 6148
  341.6 11.7 %copy-start.16 = (f32[47,512]{1,0:T(8,128)S(1)}, f32[47,512]{1,0:T(8,128)}, u32[]{:S(2)}) copy-start(f32[47,512]{1,0:T(8,128)} %slice.879) | copy-start | bytes 288772
  341.6 11.7 %copy-start.17 = (f32[47,512]{1,0:T(8,128)S(1)}, f32[47,512]{1,0:T(8,128)}, u32[]{:S(2)}) copy-start(f32[47,512]{1,0:T(8,128)} %slice.977) | copy-start | bytes 288772
  348.2 8.3 %copy-start.25 = (f32[1,512]{1,0:T(1,128)S(1)}, f32[1,512]{1,0:T(1,128)}, u32[]{:S(2)}) copy-start(f32[1,512]{1,0:T(1,128)} %slice.1071) | copy-start | bytes 6148
  354.6 9.9 %copy-start.24 = (f32[1,512]{1,0:T(1,128)S(1)}, f32[1,512]{1,0:T(1,128)}, u32[]{:S(2)}) copy-start(f32[1,512]{1,0:T(1,128)} %slice.1132) | copy-start | bytes 6148
  364.6 8.9 %copy-start.15 = (f32[95,512]{1,0:T(8,128)S(1)}, f32[95,512]{1,0:T(8,128)}, u32[]{:S(2)}) copy-start(f32[95,512]{1,0:T(8,128)} %get-tuple-element.38) | copy-start | bytes 583684
  364.6 8.9 %copy-start.23 = (f32[1,512]{1,0:T(1,128)S(1)}, f32[1,512]{1,0:T(1,128)}, u32[]{:S(2)}) copy-start(f32[1,512]{1,0:T(1,128)} %slice.1070) | copy-start | bytes 6148
  366.3 7.2 %copy-start.1 = (f32[192,512]{1,0:T(8,128)}, f32[192,512]{1,0:T(8,128)S(1)}, u32[]{:S(2)}) copy-start(f32[192,512]{1,0:T(8,128)S(1)} %pad.342) | copy-start | bytes 1179652
  382.3 7.1 %copy-start.22 = (f32[1,512]{1,0:T(1,128)S(1)}, f32[1,512]{1,0:T(1,128)}, u32[]{:S(2)}) copy-start(f32[1,512]{1,0:T(1,128)} %slice.1131) | copy-start | bytes 6148
  418.8 3.1 copy-start.11
  420.7 4.3 copy-start.12
  422.0 31.9 %copy-start.5 = (f32[384,512]{1,0:T(8,128)}, f32[384,512]{1,0:T(8,128)S(1)}, u32[]{:S(2)}) copy-start(f32[384,512]{1,0:T(8,128)S(1)} %pad.290) | copy-start | bytes 2359300
  426.9 28.8 %copy-start.6 = (f32[384,512]{1,0:T(8,128)S(1)}, f32[384,512]{1,0:T(8,128)}, u32[]{:S(2)}) copy-start(f32[384,512]{1,0:T(8,128)} %pad.345) | copy-start | bytes 2359300
  453.9 1.8 copy-start.7
  456.7 4.4 copy-start.8
  456.7 8.4 %copy-start.35 = (f32[2,512]{1,0:T(2,128)S(1)}, f32[2,512]{1,0:T(2,128)}, u32[]{:S(2)}) copy-start(f32[2,512]{1,0:T(2,128)} %param.23) | copy-start | bytes 12292
  456.7 8.5 %copy-start.10 = (bf16[384,512]{1,0:T(8,128)(2,1)S(1)}, bf16[384,512]{1,0:T(8,128)(2,1)}, u32[]{:S(2)}) copy-start(bf16[384,512]{1,0:T(8,128)(2,1)} %copy-done.9) | copy-start | bytes 1179652
  461.1 5.2 copy-start.36
  461.1 5.3 copy-start.37
  461.1 5.3 copy-start.38
  465.1 2.0 copy-start.34
  465.1 2.0 copy-start.42
  465.1 2.0 copy-start.43
  468.9 4.7 copy-start.3
  468.9 4.7 copy-start.4
Sparse Core Ops, SparseCore 0:
  8.9 21.2 all-gather.9
  32.3 45.8 all-gather.15
  80.3 47.6 all-gather.11
  129.9 58.9 all-gather.13
  190.8 48.5 all-gather.17
  479.8 52.4 reduce-scatter.1
where the time goes:
time: 550 us; the launch traced here: 541 us
  local copies, waits for them, and re-layouts  209 us (38%)
  waiting for transfers between devices  157 us (29%)
  other arithmetic  76.3 us (14%)
  blocking collectives  47.6 us (9%)
  matrix products  21.9 us (4%)
  between operations  14.9 us (3%)
  starting transfers between devices  13.9 us (3%)
    slice x118, local copies, waits for them, and re-layouts, per_device(): lax.associative_scan(link_pair, (keep_rate, drive_term), reverse=directio...  159 us
    reduce_scatter x1, waiting for transfers between devices, per_device(): lax.psum_scatter(jnp.dot(y_pool, weight_pool, preferred_element_type=jnp....  52.6 us
    all_gather x1, waiting for transfers between devices, per_device(): lax.all_gather(w_lru_in, 'sp', axis=0, tiled=True)  46.2 us
    all_gather x1, waiting for transfers between devices, per_device(): lax.all_gather(w_pool_in, 'sp', axis=0, tiled=True)  39.7 us
    mul x38, other arithmetic, link_pair(): earlier[0] * later_pair[0]  34.9 us
    pad x60, local copies, waits for them, and re-layouts, per_device(): lax.associative_scan(link_pair, (keep_rate, drive_term), reverse=directio...  31.2 us
    all_gather x1, blocking collectives, per_device(): lax.all_gather(summary_prod, 'sp', axis=0, tiled=True)  24.2 us
    all_gather x1, blocking collectives, per_device(): lax.all_gather(summary_sum, 'sp', axis=0, tiled=True)  23.3 us
  transfers between devices with their start and end apart: 10, of which 4 were waited for; matrix products, arithmetic and copies ran while one was open for 55% of the time, Pallas kernels for 0%

commit v1 on v0

v1 whole, which is shorter than its diff:
```python
import functools

import jax
import jax.numpy as jnp
from jax import lax
from jax.experimental import pallas as pl
from jax.experimental.pallas import tpu as pltpu
from jax.sharding import PartitionSpec as P

POOL_GROUPS = 4
GRID_W = 32
REACH = 2 ** (POOL_GROUPS - 1)
EPSILON = 1e-06
EDGE = 16
CHUNKS = 8


def one_minus_exp(y):
    series = jnp.full_like(y, 1.0 / 40320.0)
    for factorial in (5040.0, 720.0, 120.0, 24.0, 6.0, 2.0, 1.0):
        series = series * y + 1.0 / factorial
    return jnp.where(y > -0.35, -y * series, 1.0 - jnp.exp(y))


def pool_stage(ext, mix_ref, tp, first_row, row_count, tokens):
    half = jnp.left_shift(jnp.int32(1), tp)
    reached = ext.shape[0]
    shape = (tokens, reached)
    out_tok = lax.broadcasted_iota(jnp.int32, shape, 0)
    in_tok = lax.broadcasted_iota(jnp.int32, shape, 1)
    row_step = in_tok // GRID_W - REACH - out_tok // GRID_W
    col_step = in_tok % GRID_W - out_tok % GRID_W
    inside = (row_step >= -half) & (row_step < half) & (col_step >= -half) & (col_step < half)
    box = jnp.where(inside, 1.0, 0.0).astype(jnp.bfloat16)
    total = jnp.dot(box, ext[...], preferred_element_type=jnp.float32)
    tok = lax.broadcasted_iota(jnp.int32, (tokens, 1), 0)
    row, col = first_row + tok // GRID_W, tok % GRID_W
    rows = jnp.minimum(row + half, row_count) - jnp.maximum(row - half, 0)
    cols = jnp.minimum(col + half, GRID_W) - jnp.maximum(col - half, 0)
    count = (rows * cols).astype(jnp.float32)
    own = ext[REACH * GRID_W : REACH * GRID_W + tokens].astype(jnp.float32)
    diff = (total / count - own).astype(jnp.bfloat16)
    return jnp.dot(diff, mix_ref[0], preferred_element_type=jnp.float32).astype(jnp.bfloat16)


def gate_stage(wide, taps_ref, rec_ref, ing_ref, rate_ref, logd_ref, keep, drive, tokens):
    tap_count = taps_ref.shape[0]
    taps = taps_ref[...].astype(jnp.float32)
    left = tap_count // 2
    blocks, head = rec_ref.shape[1:3]
    for block in range(blocks):
        lanes = slice(block * head, (block + 1) * head)
        conv = wide[EDGE - left : EDGE - left + tokens, lanes] * taps[0:1, lanes]
        for k in range(1, tap_count):
            at = EDGE - left + k
            conv = conv + wide[at : at + tokens, lanes] * taps[k : k + 1, lanes]
        conv_in = conv.astype(jnp.bfloat16)
        drive_in = conv_in.astype(jnp.float32)
        for d in range(2):
            rec = jax.nn.sigmoid(
                jnp.dot(conv_in, rec_ref[d, block], preferred_element_type=jnp.float32)
            )
            ing = jax.nn.sigmoid(
                jnp.dot(conv_in, ing_ref[d, block], preferred_element_type=jnp.float32)
            )
            log_keep = -8.0 * rec * rate_ref[d : d + 1, lanes] + logd_ref[:, d : d + 1]
            keep[d * blocks + block] = jnp.exp(log_keep)
            drive[d * blocks + block] = jnp.sqrt(one_minus_exp(2.0 * log_keep)) * ing * drive_in


def scan_stage(keep, drive, tokens):
    steps = tokens // CHUNKS
    count, head = keep.shape[0], keep.shape[2]

    def step(i, carry):
        after = []
        for k in range(count):
            at = i if k < count // 2 else steps - 1 - i
            rows = pl.ds(at, CHUNKS, stride=steps)
            a = keep[k, rows, :]
            prod = a * carry[2 * k]
            state = a * carry[2 * k + 1] + drive[k, rows, :]
            keep[k, rows, :] = prod
            drive[k, rows, :] = state
            after += [prod, state]
        return tuple(after)

    one = jnp.ones((CHUNKS, head), jnp.float32)
    zero = jnp.zeros((CHUNKS, head), jnp.float32)
    out = lax.fori_loop(0, steps, step, (one, zero) * count)
    halves = (out[:count], out[count:])
    return tuple(jnp.concatenate(half[j::2], axis=1) for half in halves for j in range(2))


def run_summary(pf, hf, pb, hb):
    fp, fh = pf[0:1], hf[0:1]
    bp, bh = pb[CHUNKS - 1 :], hb[CHUNKS - 1 :]
    for c in range(1, CHUNKS):
        fh = pf[c : c + 1] * fh + hf[c : c + 1]
        fp = fp * pf[c : c + 1]
        r = CHUNKS - 1 - c
        bh = pb[r : r + 1] * bh + hb[r : r + 1]
        bp = bp * pb[r : r + 1]
    return jnp.concatenate([fp, fh, bp, bh], axis=0)


def close_stage(keep, drive, ends, enter_f, enter_b, y_ref, tokens):
    pf, hf, pb, hb = ends
    steps = tokens // CHUNKS
    fs, bs = [enter_f], [enter_b]
    for c in range(CHUNKS - 1):
        fs.append(pf[c : c + 1] * fs[-1] + hf[c : c + 1])
        r = CHUNKS - 1 - c
        bs.append(pb[r : r + 1] * bs[-1] + hb[r : r + 1])
    blocks, head = keep.shape[0] // 2, keep.shape[2]
    for c in range(CHUNKS):
        rows = slice(c * steps, (c + 1) * steps)
        for block in range(blocks):
            lanes = slice(block * head, (block + 1) * head)
            y_ref[rows, lanes] = (
                keep[block, rows, :] * fs[c][:, lanes]
                + drive[block, rows, :]
                + keep[blocks + block, rows, :] * bs[CHUNKS - 1 - c][:, lanes]
                + drive[blocks + block, rows, :]
            ).astype(jnp.bfloat16)


def local_kernel(
    ext, lru, mix, taps, rec, ing, rate, logd, y_pool, keep, drive, summary, ends, wide, *, sp
):
    tokens = y_pool.shape[0]
    grid_rows = tokens // GRID_W
    wide[...] = lru[...].astype(jnp.float32)
    gate_stage(wide, taps, rec, ing, rate, logd, keep, drive, tokens)
    parts = scan_stage(keep, drive, tokens)
    summary[...] = run_summary(*parts)
    for k in range(4):
        ends[k] = parts[k]
    y_pool[...] = pool_stage(
        ext, mix, lax.axis_index("tp"), lax.axis_index("sp") * grid_rows, sp * grid_rows, tokens
    )


def close_kernel(keep, drive, ends, enter, y_ref):
    parts = tuple(ends[k] for k in range(4))
    close_stage(keep, drive, parts, enter[0:1], enter[1:2], y_ref, y_ref.shape[0])


def with_halo(cells, width, sp):
    ends = sp - 1
    tail, head = cells[cells.shape[0] - width :], cells[:width]
    return jnp.concatenate(
        [
            lax.ppermute(tail, "sp", [(i, i + 1) for i in range(ends)]),
            cells,
            lax.ppermute(head, "sp", [(i + 1, i) for i in range(ends)]),
        ],
        axis=0,
    )


def per_device(
    sp,
    tokens,
    norm_gain,
    w_pool_in,
    w_lru_in,
    pool_mix,
    conv_taps,
    rec_gate,
    in_gate,
    decay_rate,
    log_decay,
    start_state,
    w_out_pool,
    w_out_lru,
):
    count = tokens.shape[0]
    width = w_lru_in.shape[1]
    whole = lax.all_gather(tokens, "tp", axis=1, tiled=True)
    values = whole.astype(jnp.float32)
    scale = lax.rsqrt(jnp.mean(values * values, axis=1, keepdims=True) + EPSILON)
    normed = (values * scale * norm_gain).astype(jnp.bfloat16)
    full_lru = lax.all_gather(w_lru_in, "sp", axis=0, tiled=True)
    full_pool = lax.all_gather(w_pool_in, "sp", axis=0, tiled=True)
    u_lru = jnp.dot(normed, full_lru, preferred_element_type=jnp.float32).astype(jnp.bfloat16)
    u_pool = jnp.dot(normed, full_pool, preferred_element_type=jnp.float32).astype(jnp.bfloat16)
    ext = with_halo(u_pool, REACH * GRID_W, sp)
    lru = with_halo(u_lru, EDGE, sp)
    f32 = jnp.float32
    blocks, head = rec_gate.shape[1:3]
    vmem = pl.BlockSpec(memory_space=pltpu.VMEM)
    y_pool, keep, drive, summary, ends = pl.pallas_call(
        functools.partial(local_kernel, sp=sp),
        out_shape=(
            jax.ShapeDtypeStruct((count, width), jnp.bfloat16),
            jax.ShapeDtypeStruct((2 * blocks, count, head), f32),
            jax.ShapeDtypeStruct((2 * blocks, count, head), f32),
            jax.ShapeDtypeStruct((4, width), f32),
            jax.ShapeDtypeStruct((4, CHUNKS, width), f32),
        ),
        in_specs=[vmem] * 8,
        out_specs=(vmem,) * 5,
        scratch_shapes=[pltpu.VMEM((count + 2 * EDGE, width), f32)],
        compiler_params=pltpu.CompilerParams(vmem_limit_bytes=40 * 2**20),
    )(ext, lru, pool_mix, conv_taps, rec_gate, in_gate, decay_rate, log_decay.T)
    every = lax.all_gather(summary, "sp", axis=0, tiled=False)
    me = lax.axis_index("sp")
    enter_f, enter_b = start_state[0], start_state[1]
    for s in range(sp - 1):
        r = sp - 1 - s
        enter_f = jnp.where(s < me, every[s, 0] * enter_f + every[s, 1], enter_f)
        enter_b = jnp.where(r > me, every[r, 2] * enter_b + every[r, 3], enter_b)
    y_lru = pl.pallas_call(
        close_kernel,
        out_shape=jax.ShapeDtypeStruct((count, width), jnp.bfloat16),
        in_specs=[vmem] * 4,
        out_specs=vmem,
        compiler_params=pltpu.CompilerParams(vmem_limit_bytes=40 * 2**20),
    )(keep, drive, ends, jnp.stack([enter_f, enter_b]))
    out_pool = lax.all_gather(w_out_pool, "sp", axis=1, tiled=True)
    out_lru = lax.all_gather(w_out_lru, "sp", axis=1, tiled=True)
    partial = jnp.dot(y_pool, out_pool, preferred_element_type=f32) + jnp.dot(
        y_lru, out_lru, preferred_element_type=f32
    )
    return lax.psum_scatter(
        partial.astype(jnp.bfloat16), "tp", scatter_dimension=0, tiled=True
    )


def solution(mesh):
    placed = (
        P("sp", "tp"),
        P(),
        P("sp", "tp"),
        P("sp", "tp"),
        P("tp", None, None),
        P(None, "tp"),
        P(None, "tp", None, None),
        P(None, "tp", None, None),
        P(None, "tp"),
        P(None, "sp"),
        P(None, "tp"),
        P("tp", "sp"),
        P("tp", "sp"),
    )
    return jax.shard_map(
        functools.partial(per_device, mesh.shape["sp"]),
        mesh=mesh,
        in_specs=placed,
        out_specs=P(("sp", "tp"), None),
        check_vma=False,
    )
```

time: 550 us -> 276 us (0.50); the launches traced: 541 us -> 274 us
  local copies, waits for them, and re-layouts: 209 us -> 0.23 us
  other arithmetic: 76.3 us -> 1.97 us
  waiting for transfers between devices: 157 us -> 200 us
  blocking collectives: 47.6 us -> 22.7 us
  matrix products: 21.9 us -> 14.6 us
  Pallas kernels: 0 us -> 6.59 us
    slice x152 -> x2, local copies, waits for them, and re-layouts: 163 us -> 0.04 us  [with_halo(): tail, head = (cells[cells.shape[0] - width:], cells[:width])]
    all_gather x5, waiting for transfers between devices: 101 us -> 168 us  [the longest x1 46.8 us: per_device(): out_pool = lax.all_gather(w_out_pool, 'sp', axis=1, tiled=True)]
    mul x39 -> x0, other arithmetic: 35.7 us -> none  [the longest x38 34.9 us: link_pair(): earlier[0] * later_pair[0]]
    pad x76 -> x0, local copies, waits for them, and re-layouts: 31.5 us -> none  [the longest x60 31.2 us: per_device(): lax.associative_scan(link_pair, (keep_rate, drive_term), reverse=directio...]
    reduce_scatter x1, waiting for transfers between devices: 52.6 us -> 26.1 us  [per_device(): lax.psum_scatter(partial.astype(jnp.bfloat16), 'tp', scatter_dimension=0,...]
    all_gather x2 -> x1, blocking collectives: 47.6 us -> 22.7 us  [per_device(): every = lax.all_gather(summary, 'sp', axis=0, tiled=False)]
    add x48 -> x0, other arithmetic: 16.4 us -> none  [the longest x34 15.8 us: per_device(): lax.associative_scan(link_pair, (keep_rate, drive_term), reverse=directio...]
    concatenate x41 -> x2, other arithmetic: 14.5 us -> 0.09 us  [with_halo(): jnp.concatenate([lax.ppermute(tail, 'sp', [(i, i + 1) for i in range(ends...]
  transfers between devices with their start and end apart: 10 -> 10, of which waited for: 4 -> 7; matrix products, arithmetic and copies ran while one was open for 55% -> 4% of each run, Pallas kernels for 0% -> 2%
where the time goes in v1:
time: 276 us; the launch traced here: 274 us
  waiting for transfers between devices  200 us (72%)
  blocking collectives  22.7 us (8%)
  matrix products  14.6 us (5%)
  starting transfers between devices  14 us (5%)
  between operations  13.8 us (5%)
  Pallas kernels  6.59 us (2%)
    all_gather x1, waiting for transfers between devices, per_device(): out_pool = lax.all_gather(w_out_pool, 'sp', axis=1, tiled=True)  46.8 us
    all_gather x1, waiting for transfers between devices, per_device(): full_pool = lax.all_gather(w_pool_in, 'sp', axis=0, tiled=True)  46.2 us
    all_gather x1, waiting for transfers between devices, per_device(): full_lru = lax.all_gather(w_lru_in, 'sp', axis=0, tiled=True)  43.5 us
    reduce_scatter x1, waiting for transfers between devices, per_device(): lax.psum_scatter(partial.astype(jnp.bfloat16), 'tp', scatter_dimension=0,...  26.1 us
    all_gather x1, blocking collectives, per_device(): every = lax.all_gather(summary, 'sp', axis=0, tiled=False)  22.7 us
    all_gather x1, waiting for transfers between devices, per_device(): whole = lax.all_gather(tokens, 'tp', axis=1, tiled=True)  20.2 us
    all_gather x1, waiting for transfers between devices, per_device(): out_lru = lax.all_gather(w_out_lru, 'sp', axis=1, tiled=True)  10.8 us
    ppermute x2, starting transfers between devices, with_halo(): lax.ppermute(tail, 'sp', [(i, i + 1) for i in range(ends)])  9.94 us
  transfers between devices with their start and end apart: 10, of which 7 were waited for; matrix products, arithmetic and copies ran while one was open for 4% of the time, Pallas kernels for 2%

profile of v1, /device:TPU:3, one launch (start us, length us, event | category | flops | bytes accessed | tf_op | source)
XLA Modules:
  0.0 274.0 jit_solution(12633787074007687917)
XLA Ops:
  6.5 0.0 copy-start.8
  6.5 0.0 all-gather.8.cloned.1.call-start
  6.5 0.7 all-gather.8.cloned.1.call-update
  7.3 0.0 all-gather.10.cloned.1.call-start
  7.3 0.7 all-gather.10.cloned.1.call-update
  8.0 0.0 all-gather.12.cloned.1.call-start
  8.1 0.7 all-gather.12.cloned.1.call-update
  8.7 0.0 all-gather.16.cloned.1.call-start
  8.8 0.5 all-gather.16.cloned.1.call-update
  9.3 0.0 all-gather.14.cloned.1.call-start
  9.4 0.5 all-gather.14.cloned.1.call-update
  9.9 0.0 reduce-scatter.2.cloned.1.call-start
  10.0 20.2 %all-gather.8.cloned.1.call-done = bf16[384,2048]{1,0:T(8,128)(2,1)} async-done(((bf16[384,512]{1,0:T(8,128)(2,1)}), bf16[384,2048]{1,0:T(8,128)(2,1)}) %all-gather.8.cloned.1.call-update) | async-done | bytes 1572880 | tf_op jit(solution)/shard_map/all_gather | solution.py:180
  30.2 1.8 fusion
  32.0 0.0 copy-start.5
  32.0 46.2 %all-gather.10.cloned.1.call-done = bf16[2048,512]{1,0:T(8,128)(2,1)} async-done(((bf16[256,512]{1,0:T(8,128)(2,1)}), bf16[2048,512]{1,0:T(8,128)(2,1)}) %all-gather.10.cloned.1.call-update) | async-done | bytes 2097168 | tf_op jit(solution)/shard_map/all_gather | solution.py:185
  78.2 0.0 copy-done.8
  78.2 3.1 %convolution_convert_fusion.1 = bf16[384,512]{1,0:T(8,128)(2,1)S(1)} fusion(bf16[2048,512]{1,0:T(8,128)(2,1)} %all-gather.10.cloned.1.call-done, bf16[384,2048]{1,0:T(8,128)(2,1)} %all-gather.8.cloned.1.call-done, f32[2048]{0:T(1024)S(1)} %copy-done.8, f32[384]{0:T(512)S(1)} %add_rsqrt_fusion), kind=kOutput, calls=%fused_computation.7 | convolution fusion | flops 808648704 | bytes 4072960 | tf_op jit(solution)/shard_map/dot_general | solution.py:187
  81.4 4.9 %collective-permute-start = (bf16[256,512]{1,0:T(8,128)(2,1)S(1)}, bf16[256,512]{1,0:T(8,128)(2,1)S(1)}, u32[]{:S(2)}, u32[]{:S(2)}) collective-permute-start(bf16[256,512]{1,0:T(8,128)(2,1)S(1)} %get-tuple-element.17), channel_id=1, source_target_pairs={{0,4},{4,8},{8,12},{12,16},{16,20},{20,24},{24,28},{1,5},{5,9},{9,... | collective-permute-start | bytes 786440 | tf_op jit(solution)/shard_map/ppermute | solution.py:154
  86.3 0.0 copy-start.7
  86.3 1.9 collective-permute-start.1
  88.2 43.5 %all-gather.12.cloned.1.call-done = bf16[2048,512]{1,0:T(8,128)(2,1)} async-done(((bf16[256,512]{1,0:T(8,128)(2,1)}), bf16[2048,512]{1,0:T(8,128)(2,1)}) %all-gather.12.cloned.1.call-update) | async-done | bytes 2097168 | tf_op jit(solution)/shard_map/all_gather | solution.py:184
  131.7 0.0 copy-done.5
  131.7 2.6 convolution_convert_fusion
  134.3 0.0 copy-start
  134.3 0.0 copy-start.1
  134.3 0.0 copy-start.2
  134.3 0.0 copy-start.3
  134.3 0.0 copy-start.4
  134.4 5.0 %collective-permute-start.2 = (bf16[16,512]{1,0:T(8,128)(2,1)S(1)}, bf16[16,512]{1,0:T(8,128)(2,1)S(1)}, u32[]{:S(2)}, u32[]{:S(2)}) collective-permute-start(bf16[16,512]{1,0:T(8,128)(2,1)S(1)} %get-tuple-element.15), channel_id=1, source_target_pairs={{0,4},{4,8},{8,12},{12,16},{16,20},{20,24},{24,28},{1,5},{5,9},{9,... | collective-permute-start | bytes 49160 | tf_op jit(solution)/shard_map/ppermute | solution.py:154
  139.4 1.9 collective-permute-start.3
  141.4 0.0 copy-done.7
  141.4 0.1 copy.15
  141.5 0.0 collective-permute-done.2
  141.5 3.3 %collective-permute-done.3 = bf16[16,512]{1,0:T(8,128)(2,1)S(1)} collective-permute-done((bf16[16,512]{1,0:T(8,128)(2,1)S(1)}, bf16[16,512]{1,0:T(8,128)(2,1)S(1)}, u32[]{:S(2)}, u32[]{:S(2)}) %collective-permute-start.3) | collective-permute-done | bytes 16416 | tf_op jit(solution)/shard_map/ppermute | solution.py:156
  144.9 0.0 copy-start.6
  144.9 0.0 collective-permute-done
  144.9 0.0 collective-permute-done.1
  145.0 0.1 pad_maximum_fusion.ext
  145.0 0.0 copy-done
  145.0 0.0 copy-done.1
  145.0 0.0 copy-done.2
  145.1 0.0 copy-done.3
  145.1 0.0 copy-done.4
  145.1 6.4 %shard_map.127 = (bf16[384,512]{1,0:T(8,128)(2,1)S(1)}, f32[8,384,128]{2,1,0:T(8,128)S(1)}, f32[8,384,128]{2,1,0:T(8,128)S(1)}, f32[4,512]{1,0:T(4,128)S(1)}, f32[4,8,512]{2,1,0:T(8,128)S(1)}) custom-call(bf16[896,512]{1,0:T(8,128)(2,1)S(1)} %pad_maximum_fusion.ext, bf16[416,512]{1,0:T(8,128)(2,1)S(1)} %pad_maximum_fusion.1.lru, ...), custom_call_target="tpu_custom_call" | custom-call | tf_op jit(solution)/shard_map/pallas_call | solution.py:193
  151.5 22.7 %all-gather.1 = f32[8,4,512]{2,1,0:T(4,128)S(1)} all-gather(f32[1,4,512]{2,1,0:T(4,128)S(1)} %bitcast.265), channel_id=2, replica_groups=mesh['sp'=8,'tp'=4] {'sp'}, dimensions={0}, use_global_device_ids=true | all-gather | bytes 73728 | tf_op jit(solution)/shard_map/all_gather | solution.py:207
  174.2 0.0 copy-done.6
  174.3 0.2 shard_map.128
  174.5 10.8 %all-gather.16.cloned.1.call-done = bf16[512,2048]{1,0:T(8,128)(2,1)} async-done(((bf16[512,256]{1,0:T(8,128)(2,1)}), bf16[512,2048]{1,0:T(8,128)(2,1)}) %all-gather.16.cloned.1.call-update) | async-done | bytes 2097168 | tf_op jit(solution)/shard_map/all_gather | solution.py:222
  185.3 4.3 %fusion.35 = f32[384,2048]{1,0:T(8,128)} fusion(bf16[384,512]{1,0:T(8,128)(2,1)S(1)} %shard_map.128, bf16[512,2048]{1,0:T(8,128)(2,1)} %all-gather.16.cloned.1.call-done), kind=kOutput, calls=%fused_computation.84 | convolution fusion | flops 805306368 | bytes 5636096 | tf_op jit(solution)/shard_map/dot_general | solution.py:223
  189.6 46.8 %all-gather.14.cloned.1.call-done = bf16[512,2048]{1,0:T(8,128)(2,1)} async-done(((bf16[512,256]{1,0:T(8,128)(2,1)}), bf16[512,2048]{1,0:T(8,128)(2,1)}) %all-gather.14.cloned.1.call-update) | async-done | bytes 2097168 | tf_op jit(solution)/shard_map/all_gather | solution.py:221
  236.4 4.6 %add_convert_fusion = bf16[384,2048]{1,0:T(8,128)(2,1)} fusion(f32[384,2048]{1,0:T(8,128)} %fusion.35, bf16[384,512]{1,0:T(8,128)(2,1)S(1)} %get-tuple-element.10, bf16[512,2048]{1,0:T(8,128)(2,1)} %all-gather.14.cloned.1.call-done), kind=kOutput, calls=%fused_computation.5 | convolution fusion | flops 806879232 | bytes 7208960 | tf_op jit(solution)/shard_map/dot_general | solution.py:223
  241.1 0.0 reduce-scatter.2.cloned.1.call-update
  241.1 26.1 %reduce-scatter.2.cloned.1.call-done = bf16[96,2048]{1,0:T(8,128)(2,1)} async-done(((bf16[384,2048]{1,0:T(8,128)(2,1)}), bf16[96,2048]{1,0:T(8,128)(2,1)}) %reduce-scatter.2.cloned.1.call-update) | async-done | bytes 393232 | tf_op jit(solution)/shard_map/reduce_scatter | solution.py:226
  (7 shorter events, 0.2 us)
Async XLA Ops:
  6.5 71.7 %copy-start.8 = (f32[2048]{0:T(1024)S(1)}, f32[2048]{0:T(1024)}, u32[]{:S(2)}) copy-start(f32[2048]{0:T(1024)} %param.14) | copy-start | bytes 24580
  6.5 23.6 %all-gather.8.cloned.1.call-start = ((), (), s32[]{:S(2)}) async-start(), calls=%async_computation.1 | async-start | bytes 1966080 | tf_op jit(solution)/shard_map/all_gather | solution.py:180
  7.3 70.9 %all-gather.10.cloned.1.call-start = ((), (), s32[]{:S(2)}) async-start(), calls=%async_computation.2 | async-start | bytes 2359296 | tf_op jit(solution)/shard_map/all_gather | solution.py:185
  8.0 123.7 %all-gather.12.cloned.1.call-start = ((), (), s32[]{:S(2)}) async-start(), calls=%async_computation.3 | async-start | bytes 2359296 | tf_op jit(solution)/shard_map/all_gather | solution.py:184
  8.7 176.6 %all-gather.16.cloned.1.call-start = ((), (), s32[]{:S(2)}) async-start(), calls=%async_computation.5 | async-start | bytes 2359296 | tf_op jit(solution)/shard_map/all_gather | solution.py:222
  9.3 227.1 %all-gather.14.cloned.1.call-start = ((), (), s32[]{:S(2)}) async-start(), calls=%async_computation.4 | async-start | bytes 2359296 | tf_op jit(solution)/shard_map/all_gather | solution.py:221
  9.9 257.3 %reduce-scatter.2.cloned.1.call-start = ((), (), s32[]{:S(2)}) async-start(), calls=%async_computation.6 | async-start | bytes 1966080 | tf_op jit(solution)/shard_map/reduce_scatter | solution.py:226
  32.0 99.7 %copy-start.5 = (bf16[384,2048]{1,0:T(8,128)(2,1)S(1)}, bf16[384,2048]{1,0:T(8,128)(2,1)}, u32[]{:S(2)}) copy-start(bf16[384,2048]{1,0:T(8,128)(2,1)} %all-gather.8.cloned.1.call-done) | copy-start | bytes 4718596
  81.4 63.6 %collective-permute-start = (bf16[256,512]{1,0:T(8,128)(2,1)S(1)}, bf16[256,512]{1,0:T(8,128)(2,1)S(1)}, u32[]{:S(2)}, u32[]{:S(2)}) collective-permute-start(bf16[256,512]{1,0:T(8,128)(2,1)S(1)} %get-tuple-element.17), channel_id=1, source_target_pairs={{0,4},{4,8},{8,12},{12,16},{16,20},{20,24},{24,28},{1,5},{5,9},{9,... | collective-permute-start | bytes 786440 | tf_op jit(solution)/shard_map/ppermute | solution.py:154
  86.3 55.1 %copy-start.7 = (f32[2,384]{1,0:T(2,128)S(1)}, f32[2,384]{1,0:T(2,128)}, u32[]{:S(2)}) copy-start(f32[2,384]{1,0:T(2,128)} %param.22) | copy-start | bytes 9220
  86.3 58.7 %collective-permute-start.1 = (bf16[256,512]{1,0:T(8,128)(2,1)S(1)}, bf16[256,512]{1,0:T(8,128)(2,1)S(1)}, u32[]{:S(2)}, u32[]{:S(2)}) collective-permute-start(bf16[256,512]{1,0:T(8,128)(2,1)S(1)} %get-tuple-element.18), channel_id=1, source_target_pairs={{4,0},{8,4},{12,8},{16,12},{20,16},{24,20},{28,24},{5,1},{9,5},{13... | collective-permute-start | bytes 786440 | tf_op jit(solution)/shard_map/ppermute | solution.py:156
  134.3 10.7 %copy-start = (bf16[1,512,512]{2,1,0:T(8,128)(2,1)S(1)}, bf16[1,512,512]{2,1,0:T(8,128)(2,1)}, u32[]{:S(2)}) copy-start(bf16[1,512,512]{2,1,0:T(8,128)(2,1)} %mix.1) | copy-start | bytes 1572868
  134.3 10.7 %copy-start.1 = (bf16[2,4,128,128]{3,2,1,0:T(8,128)(2,1)S(1)}, bf16[2,4,128,128]{3,2,1,0:T(8,128)(2,1)}, u32[]{:S(2)}) copy-start(bf16[2,4,128,128]{3,2,1,0:T(8,128)(2,1)} %rec.1) | copy-start | bytes 786436
  134.3 10.7 %copy-start.2 = (bf16[2,4,128,128]{3,2,1,0:T(8,128)(2,1)S(1)}, bf16[2,4,128,128]{3,2,1,0:T(8,128)(2,1)}, u32[]{:S(2)}) copy-start(bf16[2,4,128,128]{3,2,1,0:T(8,128)(2,1)} %ing.1) | copy-start | bytes 786436
  134.3 10.7 %copy-start.3 = (bf16[4,512]{1,0:T(4,128)(2,1)S(1)}, bf16[4,512]{1,0:T(4,128)(2,1)}, u32[]{:S(2)}) copy-start(bf16[4,512]{1,0:T(4,128)(2,1)} %taps.1) | copy-start | bytes 12292
  134.3 10.7 %copy-start.4 = (f32[2,512]{1,0:T(2,128)S(1)}, f32[2,512]{1,0:T(2,128)}, u32[]{:S(2)}) copy-start(f32[2,512]{1,0:T(2,128)} %rate.1) | copy-start | bytes 12292
  134.4 7.2 %collective-permute-start.2 = (bf16[16,512]{1,0:T(8,128)(2,1)S(1)}, bf16[16,512]{1,0:T(8,128)(2,1)S(1)}, u32[]{:S(2)}, u32[]{:S(2)}) collective-permute-start(bf16[16,512]{1,0:T(8,128)(2,1)S(1)} %get-tuple-element.15), channel_id=1, source_target_pairs={{0,4},{4,8},{8,12},{12,16},{16,20},{20,24},{24,28},{1,5},{5,9},{9,... | collective-permute-start | bytes 49160 | tf_op jit(solution)/shard_map/ppermute | solution.py:154
  139.4 5.5 %collective-permute-start.3 = (bf16[16,512]{1,0:T(8,128)(2,1)S(1)}, bf16[16,512]{1,0:T(8,128)(2,1)S(1)}, u32[]{:S(2)}, u32[]{:S(2)}) collective-permute-start(bf16[16,512]{1,0:T(8,128)(2,1)S(1)} %get-tuple-element.16), channel_id=1, source_target_pairs={{4,0},{8,4},{12,8},{16,12},{20,16},{24,20},{28,24},{5,1},{9,5},{13... | collective-permute-start | bytes 49160 | tf_op jit(solution)/shard_map/ppermute | solution.py:156
  144.9 29.3 %copy-start.6 = (f32[2,512]{1,0:T(2,128)S(1)}, f32[2,512]{1,0:T(2,128)}, u32[]{:S(2)}) copy-start(f32[2,512]{1,0:T(2,128)} %param.23) | copy-start | bytes 12292
Sparse Core Ops, SparseCore 0:
  8.9 21.2 all-gather.7
  32.3 45.8 all-gather.9
  80.3 51.2 all-gather.11
  133.6 51.7 all-gather.15
  187.2 49.1 all-gather.13
  241.2 25.9 reduce-scatter.1

commit v2 on v1

--- a/solution.py
+++ b/solution.py
@@ -125,42 +125,369 @@
             ).astype(jnp.bfloat16)
 
 
-def local_kernel(
-    ext, lru, mix, taps, rec, ing, rate, logd, y_pool, keep, drive, summary, ends, wide, *, sp
+def remote(src, dst, send_sem, recv_sem, axis, index):
+    return pltpu.make_async_remote_copy(
+        src_ref=src,
+        dst_ref=dst,
+        send_sem=send_sem,
+        recv_sem=recv_sem,
+        device_id={axis: index},
+        device_id_type=pl.DeviceIdType.MESH,
+    )
+
+
+class BlockGather:
+    def __init__(self, buf, sems, me, sp):
+        self.buf, self.sems = buf, sems
+        self.line = sp // 2
+        self.a, self.b = me // 2, me % 2
+
+    def copy(self, origin, other, send, recv, target):
+        block = self.buf.at[origin * 2 + other]
+        return remote(
+            block, block, self.sems.at[send, origin], self.sems.at[recv, origin], "sp", target
+        )
+
+    def right(self, o):
+        return self.copy(o, self.b, 0, 3, (self.a + 1) * 2 + self.b)
+
+    def left(self, o):
+        return self.copy(o, self.b, 1, 3, (self.a - 1) * 2 + self.b)
+
+    def across(self, o):
+        return self.copy(o, self.b, 2, 4, self.a * 2 + 1 - self.b)
+
+    def landed(self, o):
+        return self.copy(o, 1 - self.b, 2, 4, self.a * 2 + 1 - self.b)
+
+    def start(self):
+        a = self.a
+
+        @pl.when(a < self.line - 1)
+        def _():
+            self.right(a).start()
+
+        @pl.when(a > 0)
+        def _():
+            self.left(a).start()
+
+        self.across(a).start()
+
+    def step(self, d):
+        a, line = self.a, self.line
+        low, high = a - d, a + d
+
+        @pl.when(low >= 0)
+        def _():
+            self.right(low).wait_recv()
+
+            @pl.when(a < line - 1)
+            def _():
+                self.right(low).start()
+
+            self.across(low).start()
+
+        @pl.when(high < line)
+        def _():
+            self.left(high).wait_recv()
+
+            @pl.when(a > 0)
+            def _():
+                self.left(high).start()
+
+            self.across(high).start()
+
+    def both(self, d, use, wait=False, other=None):
+        a = self.a
+        side = self.b if other is None else other
+        for origin, there in ((a - d, a - d >= 0), (a + d, (a + d < self.line) & (d > 0))):
+
+            @pl.when(there)
+            def _(origin=origin):
+                if wait:
+                    self.landed(origin).wait_recv()
+                use(origin * 2 + side)
+
+    def finish(self):
+        a, line = self.a, self.line
+
+        @pl.loop(0, line)
+        def _(o):
+            @pl.when((o <= a) & (a < line - 1))
+            def _():
+                self.right(o).wait_send()
+
+            @pl.when((o >= a) & (a > 0))
+            def _():
+                self.left(o).wait_send()
+
+            self.across(o).wait_send()
+
+
+def layer_kernel(
+    tok,
+    gain,
+    wpi,
+    wli,
+    mix,
+    taps,
+    rec,
+    ing,
+    rate,
+    logd,
+    start,
+    wpo,
+    wlo,
+    out,
+    toks,
+    normed,
+    win,
+    wout,
+    acc,
+    ext,
+    edge,
+    ulru,
+    wide,
+    keep,
+    drive,
+    mine,
+    sums,
+    y_pool,
+    y_lru,
+    part,
+    red,
+    own_sem,
+    tok_sem,
+    in_sem,
+    out_sem,
+    halo_sem,
+    sum_sem,
+    red_sem,
+    *,
+    sp,
+    tp,
 ):
-    tokens = y_pool.shape[0]
-    grid_rows = tokens // GRID_W
-    wide[...] = lru[...].astype(jnp.float32)
-    gate_stage(wide, taps, rec, ing, rate, logd, keep, drive, tokens)
-    parts = scan_stage(keep, drive, tokens)
-    summary[...] = run_summary(*parts)
-    for k in range(4):
-        ends[k] = parts[k]
-    y_pool[...] = pool_stage(
-        ext, mix, lax.axis_index("tp"), lax.axis_index("sp") * grid_rows, sp * grid_rows, tokens
-    )
-
-
-def close_kernel(keep, drive, ends, enter, y_ref):
-    parts = tuple(ends[k] for k in range(4))
-    close_stage(keep, drive, parts, enter[0:1], enter[1:2], y_ref, y_ref.shape[0])
-
-
-def with_halo(cells, width, sp):
-    ends = sp - 1
-    tail, head = cells[cells.shape[0] - width :], cells[:width]
-    return jnp.concatenate(
-        [
-            lax.ppermute(tail, "sp", [(i, i + 1) for i in range(ends)]),
-            cells,
-            lax.ppermute(head, "sp", [(i + 1, i) for i in range(ends)]),
-        ],
-        axis=0,
-    )
+    f32 = jnp.float32
+    me, t = lax.axis_index("sp"), lax.axis_index("tp")
+    count, local = tok.shape
+    depth, wide_out = wpi.shape[0], wpo.shape[1]
+    share = count // tp
+    halo = REACH * GRID_W
+
+    owns = [
+        pltpu.make_async_copy(src, dst, own_sem.at[k])
+        for k, (src, dst) in enumerate(
+            (
+                (wpi, win.at[me, 0]),
+                (wli, win.at[me, 1]),
+                (tok, toks.at[t]),
+                (wpo, wout.at[me, 0]),
+                (wlo, wout.at[me, 1]),
+            )
+        )
+    ]
+    for own in owns:
+        own.start()
+
+    def tok_copy(k, source, target):
+        return remote(tok, toks.at[source], tok_sem.at[0, k], tok_sem.at[1, k], "tp", target)
+
+    for k in range(1, tp):
+        tok_copy(k, t, lax.rem(t + k, tp)).start()
+    owns[0].wait()
+    owns[1].wait()
+    first = BlockGather(win, in_sem, me, sp)
+    line = first.line
+    first.start()
+    early = min(3, line)
+    for d in range(1, early):
+        first.step(d)
+
+    owns[2].wait()
+    for k in range(1, tp):
+        source = lax.rem(t - k + tp, tp)
+        tok_copy(k, source, source).wait_recv()
+    square = jnp.zeros((count, 1), f32)
+    for p in range(tp):
+        v = toks[p].astype(f32)
+        square = square + jnp.sum(v * v, axis=1, keepdims=True)
+    scale = lax.rsqrt(square / (tp * local) + EPSILON)
+    for p in range(tp):
+        for q in range(local // depth):
+            v = toks[p, :, q * depth : (q + 1) * depth].astype(f32)
+            at = p * local + q * depth
+            normed[p * (local // depth) + q] = (
+                v * scale * gain[:, at : at + depth]
+            ).astype(jnp.bfloat16)
+
+    acc[...] = jnp.zeros_like(acc)
+
+    def use_in(block):
+        for j in range(2):
+            acc[j] += jnp.dot(normed[block], win[block, j], preferred_element_type=f32)
+
+    @pl.loop(0, early)
+    def _(d):
+        first.both(d, use_in)
+
+    @pl.loop(early, line)
+    def _(d):
+        first.step(d)
+        first.both(d, use_in)
+
+    @pl.loop(0, line)
+    def _(d):
+        first.both(d, use_in, wait=True, other=1 - first.b)
+
+    ext[halo : halo + count] = acc[0].astype(jnp.bfloat16)
+    ulru[...] = acc[1].astype(jnp.bfloat16)
+
+    def to_next(part_of):
+        if part_of == 0:
+            src, dst = ext.at[pl.ds(count, halo)], ext.at[pl.ds(0, halo)]
+        else:
+            src, dst = ulru.at[pl.ds(count - EDGE, EDGE)], edge.at[0]
+        return remote(src, dst, halo_sem.at[0, part_of], halo_sem.at[1, part_of], "sp", me + 1)
+
+    def to_prev(part_of):
+        k = 2 + part_of
+        if part_of == 0:
+            src, dst = ext.at[pl.ds(halo, halo)], ext.at[pl.ds(halo + count, halo)]
+        else:
+            src, dst = ulru.at[pl.ds(0, EDGE)], edge.at[1]
+        return remote(src, dst, halo_sem.at[0, k], halo_sem.at[1, k], "sp", me - 1)
+
+    for part_of in (1, 0):
+
+        @pl.when(me < sp - 1)
+        def _(part_of=part_of):
+            to_next(part_of).start()
+
+        @pl.when(me > 0)
+        def _(part_of=part_of):
+            to_prev(part_of).start()
+
+    owns[3].wait()
+    owns[4].wait()
+    second = BlockGather(wout, out_sem, me, sp)
+    second.start()
+
+    @pl.when(me == 0)
+    def _():
+        edge[0] = jnp.zeros(edge.shape[1:], edge.dtype)
+        ext[0:halo] = jnp.zeros((halo, ext.shape[1]), ext.dtype)
+
+    @pl.when(me == sp - 1)
+    def _():
+        edge[1] = jnp.zeros(edge.shape[1:], edge.dtype)
+        ext[halo + count :] = jnp.zeros((halo, ext.shape[1]), ext.dtype)
+
+    def halo_wait(part_of):
+        @pl.when(me > 0)
+        def _():
+            to_next(part_of).wait_recv()
+
+        @pl.when(me < sp - 1)
+        def _():
+            to_prev(part_of).wait_recv()
+
+    halo_wait(1)
+    wide[0:EDGE] = edge[0].astype(f32)
+    wide[EDGE : EDGE + count] = ulru[...].astype(f32)
+    wide[EDGE + count :] = edge[1].astype(f32)
+    gate_stage(wide, taps, rec, ing, rate, logd, keep, drive, count)
+    ends = scan_stage(keep, drive, count)
+    mine[0:4] = run_summary(*ends)
+    mine[4:8] = jnp.zeros((4, mine.shape[1]), f32)
+    sums[me] = mine[...]
+
+    def sum_copy(k, source, target):
+        return remote(mine, sums.at[source], sum_sem.at[0, k], sum_sem.at[1, k], "sp", target)
+
+    for k in range(1, sp):
+        sum_copy(k, me, lax.rem(me + k, sp)).start()
+    halo_wait(0)
+    grid_rows = count // GRID_W
+    y_pool[...] = pool_stage(ext, mix, t, me * grid_rows, sp * grid_rows, count)
+    if line > 1:
+        second.step(1)
+    for k in range(1, sp):
+        source = lax.rem(me - k + sp, sp)
+        sum_copy(k, source, source).wait_recv()
+    enter_f, enter_b = start[0:1], start[1:2]
+    for s in range(sp - 1):
+        r = sp - 1 - s
+        enter_f = jnp.where(s < me, sums[s, 0:1] * enter_f + sums[s, 1:2], enter_f)
+        enter_b = jnp.where(r > me, sums[r, 2:3] * enter_b + sums[r, 3:4], enter_b)
+    close_stage(keep, drive, ends, enter_f, enter_b, y_lru, count)
+
+    def red_copy(k, block, target):
+        rows = pl.ds(pl.multiple_of(target * share, share), share)
+        return remote(
+            part.at[block, rows],
+            red.at[k, block],
+            red_sem.at[0, k, block],
+            red_sem.at[1, k, block],
+            "tp",
+            target,
+        )
+
+    def use_out(block):
+        part[block] = (
+            jnp.dot(y_pool[...], wout[block, 0], preferred_element_type=f32)
+            + jnp.dot(y_lru[...], wout[block, 1], preferred_element_type=f32)
+        ).astype(jnp.bfloat16)
+        for k in range(1, tp):
+            red_copy(k, block, lax.rem(t + k, tp)).start()
+
+    ready = min(2, line)
+
+    @pl.loop(0, ready)
+    def _(d):
+        second.both(d, use_out)
+
+    @pl.loop(ready, line)
+    def _(d):
+        second.step(d)
+        second.both(d, use_out)
+
+    @pl.loop(0, line)
+    def _(d):
+        second.both(d, use_out, wait=True, other=1 - second.b)
+
+    rows = pl.ds(pl.multiple_of(t * share, share), share)
+    for block in range(sp):
+        total = part[block, rows, :].astype(f32)
+        for k in range(1, tp):
+            red_copy(k, block, lax.rem(t + k, tp)).wait_recv()
+            total = total + red[k, block].astype(f32)
+        out[:, block * wide_out : (block + 1) * wide_out] = total.astype(out.dtype)
+
+    first.finish()
+    second.finish()
+    for k in range(1, tp):
+        tok_copy(k, t, lax.rem(t + k, tp)).wait_send()
+    for k in range(1, sp):
+        sum_copy(k, me, lax.rem(me + k, sp)).wait_send()
+    for part_of in range(2):
+
+        @pl.when(me < sp - 1)
+        def _(part_of=part_of):
+            to_next(part_of).wait_send()
+
+        @pl.when(me > 0)
+        def _(part_of=part_of):
+            to_prev(part_of).wait_send()
+
+    @pl.loop(0, sp)
+    def _(block):
+        for k in range(1, tp):
+            red_copy(k, block, lax.rem(t + k, tp)).wait_send()
 
 
 def per_device(
     sp,
+    tp,
     tokens,
     norm_gain,
     w_pool_in,
@@ -175,56 +502,63 @@
     w_out_pool,
     w_out_lru,
 ):
-    count = tokens.shape[0]
-    width = w_lru_in.shape[1]
-    whole = lax.all_gather(tokens, "tp", axis=1, tiled=True)
-    values = whole.astype(jnp.float32)
-    scale = lax.rsqrt(jnp.mean(values * values, axis=1, keepdims=True) + EPSILON)
-    normed = (values * scale * norm_gain).astype(jnp.bfloat16)
-    full_lru = lax.all_gather(w_lru_in, "sp", axis=0, tiled=True)
-    full_pool = lax.all_gather(w_pool_in, "sp", axis=0, tiled=True)
-    u_lru = jnp.dot(normed, full_lru, preferred_element_type=jnp.float32).astype(jnp.bfloat16)
-    u_pool = jnp.dot(normed, full_pool, preferred_element_type=jnp.float32).astype(jnp.bfloat16)
-    ext = with_halo(u_pool, REACH * GRID_W, sp)
-    lru = with_halo(u_lru, EDGE, sp)
-    f32 = jnp.float32
+    count, local = tokens.shape
+    depth, width = w_lru_in.shape
+    wide_out = w_out_pool.shape[1]
     blocks, head = rec_gate.shape[1:3]
+    f32, bf16 = jnp.float32, jnp.bfloat16
     vmem = pl.BlockSpec(memory_space=pltpu.VMEM)
-    y_pool, keep, drive, summary, ends = pl.pallas_call(
-        functools.partial(local_kernel, sp=sp),
-        out_shape=(
-            jax.ShapeDtypeStruct((count, width), jnp.bfloat16),
-            jax.ShapeDtypeStruct((2 * blocks, count, head), f32),
-            jax.ShapeDtypeStruct((2 * blocks, count, head), f32),
-            jax.ShapeDtypeStruct((4, width), f32),
-            jax.ShapeDtypeStruct((4, CHUNKS, width), f32),
+    far = pl.BlockSpec(memory_space=pl.ANY)
+    share = count // tp
+    dma = pltpu.SemaphoreType.DMA
+    return pl.pallas_call(
+        functools.partial(layer_kernel, sp=sp, tp=tp),
+        out_shape=jax.ShapeDtypeStruct((share, wide_out * sp), bf16),
+        in_specs=[far, vmem, far, far] + [vmem] * 7 + [far, far],
+        out_specs=vmem,
+        scratch_shapes=[
+            pltpu.VMEM((tp, count, local), bf16),
+            pltpu.VMEM((sp, count, depth), bf16),
+            pltpu.VMEM((sp, 2, depth, width), bf16),
+            pltpu.VMEM((sp, 2, width, wide_out), bf16),
+            pltpu.VMEM((2, count, width), f32),
+            pltpu.VMEM((count + 2 * REACH * GRID_W, width), bf16),
+            pltpu.VMEM((2, EDGE, width), bf16),
+            pltpu.VMEM((count, width), bf16),
+            pltpu.VMEM((count + 2 * EDGE, width), f32),
+            pltpu.VMEM((2 * blocks, count, head), f32),
+            pltpu.VMEM((2 * blocks, count, head), f32),
+            pltpu.VMEM((8, width), f32),
+            pltpu.VMEM((sp, 8, width), f32),
+            pltpu.VMEM((count, width), bf16),
+            pltpu.VMEM((count, width), bf16),
+            pltpu.VMEM((sp, count, wide_out), bf16),
+            pltpu.VMEM((tp, sp, share, wide_out), bf16),
+            dma((5,)),
+            dma((2, tp)),
+            dma((5, sp // 2)),
+            dma((5, sp // 2)),
+            dma((2, 4)),
+            dma((2, sp)),
+            dma((2, tp, sp)),
+        ],
+        compiler_params=pltpu.CompilerParams(
+            has_side_effects=True, vmem_limit_bytes=60 * 2**20
         ),
-        in_specs=[vmem] * 8,
-        out_specs=(vmem,) * 5,
-        scratch_shapes=[pltpu.VMEM((count + 2 * EDGE, width), f32)],
-        compiler_params=pltpu.CompilerParams(vmem_limit_bytes=40 * 2**20),
-    )(ext, lru, pool_mix, conv_taps, rec_gate, in_gate, decay_rate, log_decay.T)
-    every = lax.all_gather(summary, "sp", axis=0, tiled=False)
-    me = lax.axis_index("sp")
-    enter_f, enter_b = start_state[0], start_state[1]
-    for s in range(sp - 1):
-        r = sp - 1 - s
-        enter_f = jnp.where(s < me, every[s, 0] * enter_f + every[s, 1], enter_f)
-        enter_b = jnp.where(r > me, every[r, 2] * enter_b + every[r, 3], enter_b)
-    y_lru = pl.pallas_call(
-        close_kernel,
-        out_shape=jax.ShapeDtypeStruct((count, width), jnp.bfloat16),
-        in_specs=[vmem] * 4,
-        out_specs=vmem,
-        compiler_params=pltpu.CompilerParams(vmem_limit_bytes=40 * 2**20),
-    )(keep, drive, ends, jnp.stack([enter_f, enter_b]))
-    out_pool = lax.all_gather(w_out_pool, "sp", axis=1, tiled=True)
-    out_lru = lax.all_gather(w_out_lru, "sp", axis=1, tiled=True)
-    partial = jnp.dot(y_pool, out_pool, preferred_element_type=f32) + jnp.dot(
-        y_lru, out_lru, preferred_element_type=f32
-    )
-    return lax.psum_scatter(
-        partial.astype(jnp.bfloat16), "tp", scatter_dimension=0, tiled=True
+    )(
+        tokens,
+        norm_gain[None],
+        w_pool_in,
+        w_lru_in,
+        pool_mix,
+        conv_taps,
+        rec_gate,
+        in_gate,
+        decay_rate,
+        log_decay.T,
+        start_state,
+        w_out_pool,
+        w_out_lru,
     )
 
 
@@ -245,7 +579,7 @@
         P("tp", "sp"),
     )
     return jax.shard_map(
-        functools.partial(per_device, mesh.shape["sp"]),
+        functools.partial(per_device, mesh.shape["sp"], mesh.shape["tp"]),
         mesh=mesh,
         in_specs=placed,
         out_specs=P(("sp", "tp"), None),

time: 276 us -> 127 us (0.46)
  waiting for transfers between devices: 200 us -> 0 us
  Pallas kernels: 6.59 us -> 124 us
  blocking collectives: 22.7 us -> 0 us
  matrix products: 14.6 us -> 0 us
  starting transfers between devices: 14 us -> 0 us
  between operations: 13.8 us -> 0.01 us
  local copies, waits for them, and re-layouts: 0.23 us -> 3.27 us
    all_gather x5 -> x0, waiting for transfers between devices: 168 us -> none  [the longest x1 46.8 us: per_device(): out_pool = lax.all_gather(w_out_pool, 'sp', axis=1, tiled=True)]
    pallas_call x2 -> x1, Pallas kernels: 6.59 us -> 124 us  [per_device(): pl.pallas_call(functools.partial(layer_kernel, sp=sp, tp=tp), out_shape=j...]
    reduce_scatter x1 -> x0, waiting for transfers between devices: 26.1 us -> none  [per_device(): lax.psum_scatter(partial.astype(jnp.bfloat16), 'tp', scatter_dimension=0,...]
    all_gather x1 -> x0, blocking collectives: 22.7 us -> none  [per_device(): every = lax.all_gather(summary, 'sp', axis=0, tiled=False)]
    dot_general x4 -> x0, matrix products: 14.6 us -> none  [the longest x1 4.64 us: per_device(): jnp.dot(y_pool, out_pool, preferred_element_type=f32)]
    ppermute x4 -> x0, starting transfers between devices: 13.8 us -> none  [the longest x2 9.94 us: with_halo(): lax.ppermute(tail, 'sp', [(i, i + 1) for i in range(ends)])]
    ppermute x4 -> x0, waiting for transfers between devices: 3.35 us -> none  [the longest x2 3.35 us: with_halo(): lax.ppermute(head, 'sp', [(i + 1, i) for i in range(ends)])]
    unnamed x6 -> x0, waiting for transfers between devices: 3.16 us -> none
  transfers between devices with their start and end apart: 10 -> 0, of which waited for: 7 -> 0; matrix products, arithmetic and copies ran while one was open for 4% -> 0% of each run, Pallas kernels for 2% -> 0%
where the time goes in v2:
time: 127 us
  Pallas kernels  124 us (98%)
  local copies, waits for them, and re-layouts  3.27 us (3%)
    pallas_call x1, Pallas kernels, per_device(): pl.pallas_call(functools.partial(layer_kernel, sp=sp, tp=tp), out_shape=j...  124 us
    unnamed x2, local copies, waits for them, and re-layouts  3.27 us

profile of v2, /device:TPU:3, one launch (start us, length us, event | category | flops | bytes accessed | tf_op | source)
XLA Modules:
  0.0 127.2 jit_solution(6155222129504612430)
XLA Ops:
  0.0 1.5 %copy.14 = f32[2,384]{0,1:T(8,128)} copy(f32[2,384]{1,0:T(2,128)} %param.22) | data formatting | bytes 6144 | tf_op args[9]
  1.5 123.9 %shard_map.127 = bf16[96,2048]{1,0:T(8,128)(2,1)} custom-call(bf16[384,512]{1,0:T(8,128)(2,1)} %tok.1, f32[1,2048]{1,0:T(1,128)} %bitcast.3, bf16[256,512]{1,0:T(8,128)(2,1)} %wpi.1, bf16[256,512]{1,0:T(8,128)(2,1)} %wli.1, bf16[1,512,512]{2,1,0:T(8,128)(2,1)} %mix.1, bf16[4,512]{1,0:T(4,128)(2,1)} %taps.1, bf16[2,4,128,128]{3,2,1,0:T(8,128)(2,1)} %rec.1, ...), custom_call_target="tpu_custom_call" | custom-call | tf_op jit(solution)/shard_map/pallas_call | solution.py:514
  125.4 1.8 %copy.16 = bf16[96,2048]{1,0:T(8,128)(2,1)} copy(bf16[96,2048]{1,0:T(8,128)(2,1)} %shard_map.127) | data formatting | bytes 786432
